TPU v7x, 256 devices: a 4x2x16 block of a 4x16x16 slice. The times are simulated.
256 devices in a mesh: grp: 2 (over y), sp: 32 (over z, core), tp: 4 (over x).
Axes of the slice: x: 4, y: 2, z: 16, core: 2. Of those that a mesh axis runs over, the one named last changes fastest.
The devices are a block of a 4x16x16 slice.
Arguments:
- residual_in: bfloat16 [16384, 2048], P(('grp', 'sp', 'tp')), parts along dimension 0, may hold values from -1.1953125 to 1.1953125
- query_small: bfloat16 [16384, 1024], P(('grp', 'sp'), 'tp'), parts along dimension 0, may hold values from -6 to 6
- query_large: bfloat16 [16384, 1024], P(('grp', 'sp'), 'tp'), parts along dimension 0, may hold values from -6 to 6
- key_small: bfloat16 [64, 16384], P(None, ('grp', 'sp')), parts along dimension 1, may hold values from -6 to 6
- key_large: bfloat16 [128, 16384], P(None, ('grp', 'sp')), parts along dimension 1, may hold values from -6 to 6
- value_small: bfloat16 [64, 16384], P(None, ('grp', 'sp')), parts along dimension 1, may hold values from -6 to 6
- value_large: bfloat16 [128, 16384], P(None, ('grp', 'sp')), parts along dimension 1, may hold values from -6 to 6
- forget_small: float32 [16, 16384], P('tp', ('grp', 'sp')), parts along dimension 1, may hold values from -1172 to 0, as said below
- forget_large: float32 [8, 16384], P('tp', ('grp', 'sp')), parts along dimension 1, may hold values from -1172 to 0, as said below
- project_small: bfloat16 [1024, 2048], P('tp'), may hold values from -0.125 to 0.125
- project_large: bfloat16 [1024, 2048], P('tp'), may hold values from -0.125 to 0.125
- norm_gain: bfloat16 [2048], replicated, may hold values from 0.099609375 to 1.8984375
- expert_gate: bfloat16 [128, 2048, 512], P(('sp', 'tp')), may hold values from -0.125 to 0.125
- expert_up: bfloat16 [128, 2048, 512], P(('sp', 'tp')), may hold values from -0.125 to 0.125
- expert_down: bfloat16 [128, 512, 2048], P(('sp', 'tp')), may hold values from -0.25 to 0.25
- routing: int32 [16384, 2], P(('grp', 'sp', 'tp')), parts along dimension 0, may hold values from 0 to 127, all different within a row; in each aligned block of 64 rows (0 to 63, 64 to 127, ...) at most 2 rows name the same one
- route_weight: float32 [16384, 2], P(('grp', 'sp', 'tp')), parts along dimension 0, may hold values from 0.2 to 1
Outputs:
- layer_out: bfloat16 [16384, 2048], P(('grp', 'sp', 'tp')), parts along dimension 0
There are 2 independent parts, one for each index of `grp`. A program takes and returns all parts, laid end to end along the dimension named above; an argument that names none is the same for every part. Nothing has to cross between parts.
Inputs may be any that keep to these rules, and one draw needn't show every extreme that they name: `forget_small`: each row never rises from one position to the next. `forget_large`: each row never rises from one position to the next. `routing`: each row names 2 different experts; in the rows of one device no expert is named by more than 2 rows, and in some devices' rows some expert is named by exactly 2.
All inputs are finite; a program needn't handle non-finite values.
Results may differ from a plain program's by a relative error of at most 0.018.
Values may be sent and summed in bfloat16 or wider, within the bound.
No kernel may reach another device: no remote copies, remote signals or barrier semaphores. Data moves between devices by JAX's collectives and lax.ppermute only.
A program may use at most 64 MiB of HBM per device.

v0:
```python
import math

import jax
import jax.numpy as jnp
from jax import lax
from jax.experimental import pallas as pl
from jax.experimental.pallas import tpu as pltpu
from jax.sharding import PartitionSpec as P


BF = jnp.bfloat16
F32 = jnp.float32
LOG2E = math.log2(math.e)
GATE_ROWS = 16
PIECES = 3
LOW = -1e30


def params(mib=16):
    return pltpu.CompilerParams(vmem_limit_bytes=mib << 20)


def packed(keys_values, gates, size_s, size_l, heads_s):
    at_l = size_s + GATE_ROWS
    at_v = at_l + size_l + GATE_ROWS

    def body(kv, gate, out):
        def pieces(left, size):
            left = left * -(size**0.5)
            rows = []
            for _ in range(PIECES):
                piece = left.astype(BF).astype(F32)
                rows.append(piece)
                left = left - piece
            used = PIECES * left.shape[0]
            rows.append(jnp.zeros((GATE_ROWS - used, left.shape[1]), F32))
            return jnp.concatenate(rows, axis=0).astype(BF)

        out[:size_s] = kv[:size_s]
        out[size_s:at_l] = pieces(gate[:heads_s], size_s)
        out[at_l : at_l + size_l] = kv[size_s : size_s + size_l]
        out[at_l + size_l : at_v] = pieces(gate[heads_s:], size_l)
        out[at_v:] = kv[size_s + size_l :]

    return pl.pallas_call(
        body,
        out_shape=jax.ShapeDtypeStruct((at_v + size_s + size_l, keys_values.shape[1]), BF),
        compiler_params=params(),
        name="packed",
    )(keys_values, gates)


def update(units, kind, keys, values, state, factor, keeps):
    rows = values.shape[1]
    tops = [state[g, h, rows : rows + 1] for _, g, h in units]

    def scores(i):
        queries, g, h = units[i]
        s = jnp.dot(keys[kind], queries[h], preferred_element_type=F32)
        return s if keeps is None else jnp.where(keeps[g], s, LOW)

    s = scores(0)
    for i, (_, g, h) in enumerate(units):
        following = scores(i + 1) if i + 1 < len(units) else None
        new = jnp.maximum(tops[i], jnp.max(s, axis=0, keepdims=True))
        p = jnp.exp2((s - new) * factor).astype(BF)
        alpha = jnp.exp2((tops[i] - new) * factor)
        mixed = jnp.dot(values[kind], p, preferred_element_type=F32)
        state[g, h, :rows] = state[g, h, :rows] * alpha + mixed
        state[g, h, rows:] = jnp.broadcast_to(new, (state.shape[2] - rows, new.shape[1]))
        s = following


def lay_out(blocks, keys, values, sizes):
    large = max(sizes)
    count = blocks[0].shape[1]
    at_k, at_v = 0, sum(sizes) + GATE_ROWS * len(sizes)
    for kind, size in enumerate(sizes):
        blank = jnp.zeros((large - size, count), BF)
        ones = jnp.ones((GATE_ROWS, count), BF)
        for i, block in enumerate(blocks):
            at = pl.ds(i * count, count)
            key, gates = block[at_k : at_k + size], block[at_k + size : at_k + size + GATE_ROWS]
            value = block[at_v : at_v + size]
            gap = [blank] if size < large else []
            keys[kind, at] = jnp.concatenate([key] + gap + [gates], axis=0).T
            values[kind, :, at] = jnp.concatenate([value] + gap + [ones], axis=0)
        at_k += size + GATE_ROWS
        at_v += size


def add_keys(groups, counts, sizes, keys, values, state, keeps=None, together=2):
    number = math.gcd(together, *counts)

    def some(i, carry):
        large = i * number >= counts[0]
        factor = jnp.where(large, LOG2E * sizes[1] ** -0.5, LOG2E * sizes[0] ** -0.5)
        units = [(queries, g, i * number + k) for k in range(number) for g, queries in enumerate(groups)]
        update(units, large.astype(jnp.int32), keys, values, state, factor, keeps)
        return carry

    lax.fori_loop(0, sum(counts) // number, some, 0)


def key_scratch(sizes, count):
    rows = max(sizes) + GATE_ROWS
    return [pltpu.VMEM((len(sizes), count, rows), BF), pltpu.VMEM((len(sizes), rows, count), BF)]


def first(info, own, peer, block, counts, sizes):
    tokens = own.shape[0]
    rows = max(sizes) + GATE_ROWS

    def body(info, own, peer, block, q_own, q_peer, state, keys, values):
        def spread(queries, out):
            at = h = 0
            for count, size in zip(counts, sizes):
                turned = queries[:, at : at + count * size].T
                row = lax.broadcasted_iota(jnp.int32, (GATE_ROWS, tokens), 0)
                for k in range(count):
                    chosen = (row % count == k) & (row < PIECES * count)
                    out[h, :size] = turned[k * size : (k + 1) * size]
                    if size < rows - GATE_ROWS:
                        out[h, size : rows - GATE_ROWS] = jnp.zeros((rows - GATE_ROWS - size, tokens), BF)
                    out[h, rows - GATE_ROWS :] = jnp.where(chosen, 1.0, 0.0).astype(BF)
                    h += 1
                at += count * size

        lay_out([block], keys, values, sizes)
        spread(own, q_own)
        spread(peer, q_peer)
        state[:, :, :rows] = jnp.zeros(state.shape[:2] + (rows, tokens), F32)
        state[:, :, rows:] = jnp.full(state.shape[:2] + (8, tokens), LOW, F32)
        shape = (block.shape[1], tokens)
        ahead = lax.broadcasted_iota(jnp.int32, shape, 1) - lax.broadcasted_iota(jnp.int32, shape, 0)
        keeps = [ahead >= 0, ahead >= jnp.where(info[0] == 1, -shape[0], shape[1])]
        add_keys([q_own, q_peer], counts, sizes, keys, values, state, keeps)

    vm = pl.BlockSpec(memory_space=pltpu.VMEM)
    heads = sum(counts)
    return pl.pallas_call(
        body,
        in_specs=[pl.BlockSpec(memory_space=pltpu.SMEM)] + [vm] * 3,
        out_specs=[vm] * 3,
        out_shape=[
            jax.ShapeDtypeStruct((heads, rows, tokens), BF),
            jax.ShapeDtypeStruct((heads, rows, tokens), BF),
            jax.ShapeDtypeStruct((2, heads, rows + 8, tokens), F32),
        ],
        scratch_shapes=key_scratch(sizes, block.shape[1]),
        compiler_params=params(),
        name="first",
    )(info, own, peer, block)


def advance(info, step, q_own, q_peer, blocks, state, counts, sizes):
    def body(flags, q_own, q_peer, *refs):
        arrived, state, keys, values = refs[: len(blocks)], refs[-3], refs[-2], refs[-1]

        @pl.when(flags[step] == 1)
        def _():
            lay_out(arrived, keys, values, sizes)
            add_keys([q_own, q_peer], counts, sizes, keys, values, state)

    vm = pl.BlockSpec(memory_space=pltpu.VMEM)
    return pl.pallas_call(
        body,
        in_specs=[pl.BlockSpec(memory_space=pltpu.SMEM)] + [vm] * (3 + len(blocks)),
        out_specs=vm,
        out_shape=jax.ShapeDtypeStruct(state.shape, state.dtype),
        input_output_aliases={3 + len(blocks): 0},
        scratch_shapes=key_scratch(sizes, sum(b.shape[1] for b in blocks)),
        compiler_params=params(),
    )(info, q_own, q_peer, *blocks, state)


def finish(state, got, project_s, project_l, counts, sizes):
    def body(state, got, project_s, project_l, out):
        rows = state.shape[2] - 8
        total, h = None, 0
        for count, size, project in zip(counts, sizes, (project_s, project_l)):
            factor = LOG2E * size**-0.5
            done = []
            for _ in range(count):
                a, b = state[0, h, rows : rows + 1], got[h, rows : rows + 1]
                top = jnp.maximum(a, b)
                wa, wb = jnp.exp2((a - top) * factor), jnp.exp2((b - top) * factor)
                norm = state[0, h, rows - 1 : rows] * wa + got[h, rows - 1 : rows] * wb
                done.append(((state[0, h, :size] * wa + got[h, :size] * wb) / norm).astype(BF))
                h += 1
            part = jnp.dot(jnp.concatenate(done, axis=0).T, project[...], preferred_element_type=F32)
            total = part if total is None else total + part
        out[...] = total.astype(BF)

    return pl.pallas_call(
        body,
        out_shape=jax.ShapeDtypeStruct((state.shape[3], project_s.shape[1]), BF),
        compiler_params=params(),
        name="finish",
    )(state, got, project_s, project_l)


def attend_and_project(qs, ql, key_small, key_large, value_small, value_large, gs, gl, ps, pb):
    devices = lax.axis_size("sp")
    chips = devices // 2
    place = lax.axis_index("sp").astype(jnp.int32)
    chip, core = place // 2, place % 2
    swap = [(i, i ^ 1) for i in range(devices)]
    ring = [(i, (i + 2 - 4 * (i % 2)) % devices) for i in range(devices)]
    steps = chips // 2
    k = jnp.arange(1, steps + 1, dtype=jnp.int32)
    usable = jnp.where(core == 0, chip >= k, chip + k >= chips).astype(jnp.int32)
    info = jnp.concatenate([(1 - core).reshape(1), usable])
    counts = (gs.shape[0], gl.shape[0])
    sizes = (key_small.shape[0], key_large.shape[0])

    kv = jnp.concatenate([key_small, key_large, value_small, value_large], axis=0)
    gates = jnp.concatenate([gs, gl], axis=0)
    block = packed(kv, gates, *sizes, counts[0])
    own = jnp.concatenate([qs, ql], axis=1)
    peer = lax.ppermute(own, "sp", swap)
    b = lax.ppermute(block, "sp", swap)
    a = block
    q_own, q_peer, state = first(info, own, peer, block, counts, sizes)
    for step in range(1, steps + 1):
        a = lax.ppermute(a, "sp", ring)
        blocks = [a]
        if step < steps or chips % 2:
            b = lax.ppermute(b, "sp", ring)
            blocks.append(b)
        state = advance(info, step, q_own, q_peer, blocks, state, counts, sizes)
    got = lax.ppermute(state[1], "sp", swap)
    return finish(state, got, ps, pb, counts, sizes)


def mix_body(parts, residual_in, gain, slots, resid_out, outgoing):
    projected = parts[0].astype(F32)
    for i in range(1, parts.shape[0]):
        projected = projected + parts[i].astype(F32)
    resid = residual_in[...].astype(F32) + projected
    resid_out[...] = resid
    scale = lax.rsqrt(jnp.mean(resid * resid, axis=1, keepdims=True) + 1e-06)
    normed = (resid * scale * gain[...].astype(F32)).astype(BF)
    outgoing[...] = jnp.dot(slots[...], normed, preferred_element_type=F32).astype(BF)


def mix(parts, residual_in, gain, slots):
    rows, width = residual_in.shape
    return pl.pallas_call(
        mix_body,
        out_shape=(
            jax.ShapeDtypeStruct((rows, width), F32),
            jax.ShapeDtypeStruct((slots.shape[0], width), BF),
        ),
        compiler_params=params(),
        name="mix",
    )(parts, residual_in, gain, slots)


def expert(rows, gate, up, down):
    count, width = rows.shape
    units = gate.shape[2]
    pieces = 4
    deep = width // pieces
    span = math.gcd(width, 512)

    def body(rows, gate, up, down, out, gate_v, up_v, down_v, g, u, hidden, sems):
        def inward(i):
            at = pl.ds(pl.multiple_of(i * deep, deep), deep)
            return (
                pltpu.make_async_copy(gate.at[0, at], gate_v.at[at], sems.at[2 * i]),
                pltpu.make_async_copy(up.at[0, at], up_v.at[at], sems.at[2 * i + 1]),
            )

        outward = pltpu.make_async_copy(down.at[0], down_v, sems.at[2 * pieces])
        for i in range(pieces):
            for copy in inward(i):
                copy.start()
        outward.start()
        g[...] = jnp.zeros_like(g)
        u[...] = jnp.zeros_like(u)

        def first_products(i, carry):
            at = pl.ds(pl.multiple_of(i * deep, deep), deep)
            for copy, weight, total in zip(inward(i), (gate_v, up_v), (g, u)):
                copy.wait()
                total[...] += jnp.dot(rows[:, at], weight[at], preferred_element_type=F32)
            return carry

        lax.fori_loop(0, pieces, first_products, 0)
        gated = g[...]
        hidden[...] = (gated / (1.0 + jnp.exp(-gated)) * u[...]).astype(BF)
        outward.wait()

        def last_product(i, carry):
            at = pl.ds(pl.multiple_of(i * span, span), span)
            out[:, at] = jnp.dot(hidden[...], down_v[:, at], preferred_element_type=F32).astype(BF)
            return carry

        lax.fori_loop(0, width // span, last_product, 0)

    vm = pl.BlockSpec(memory_space=pltpu.VMEM)
    return pl.pallas_call(
        body,
        in_specs=[vm] + [pl.BlockSpec(memory_space=pltpu.HBM)] * 3,
        out_specs=vm,
        out_shape=jax.ShapeDtypeStruct((count, width), BF),
        scratch_shapes=[
            pltpu.VMEM((width, units), BF),
            pltpu.VMEM((width, units), BF),
            pltpu.VMEM((units, width), BF),
            pltpu.VMEM((count, units), F32),
            pltpu.VMEM((count, units), F32),
            pltpu.VMEM((count, units), BF),
            pltpu.SemaphoreType.DMA((2 * pieces + 1,)),
        ],
        compiler_params=params(51),
        name="expert",
    )(rows, gate, up, down)


def collect_body(returned, weights, resid, out):
    total = resid[...]
    for i in range(weights.shape[0]):
        total = total + jnp.dot(weights[i], returned[...], preferred_element_type=F32)
    out[...] = total.astype(BF)


def collect(returned, weights, resid):
    return pl.pallas_call(
        collect_body,
        out_shape=jax.ShapeDtypeStruct(resid.shape, BF),
        compiler_params=params(),
        name="collect",
    )(returned, weights, resid)


def three_pieces(value):
    pieces = []
    for _ in range(PIECES):
        piece = lax.reduce_precision(value, 8, 7)
        pieces.append(piece.astype(BF))
        value = value - piece
    return jnp.stack(pieces)


def shards(
    residual_in,
    query_small,
    query_large,
    key_small,
    key_large,
    value_small,
    value_large,
    forget_small,
    forget_large,
    project_small,
    project_large,
    norm_gain,
    expert_gate,
    expert_up,
    expert_down,
    routing,
    route_weight,
):
    head_devices = lax.axis_size("tp")
    experts = lax.axis_size("sp") * head_devices
    own_rows, width = residual_in.shape
    top_count = routing.shape[1]

    partial = attend_and_project(
        query_small,
        query_large,
        key_small,
        key_large,
        value_small,
        value_large,
        forget_small,
        forget_large,
        project_small,
        project_large,
    )

    capacity = max(2, 2 * own_rows * top_count // experts)
    pairs = own_rows * top_count
    pair_expert = routing.reshape(-1)
    same = pair_expert[:, None] == pair_expert[None, :]
    before = jnp.arange(pairs)[:, None] > jnp.arange(pairs)[None, :]
    slot = jnp.sum((same & before).astype(jnp.int32), axis=1)
    target = (pair_expert * capacity + slot).reshape(own_rows, top_count)
    hit = target[:, :, None] == jnp.arange(experts * capacity)[None, None, :]
    slots = jnp.any(hit, axis=1).T.astype(BF)
    weights = three_pieces(jnp.sum(jnp.where(hit, route_weight[:, :, None], 0.0), axis=1))

    parts = partial.reshape(head_devices, own_rows, width)
    parts = lax.all_to_all(parts, "tp", split_axis=0, concat_axis=0, tiled=True)
    resid, outgoing = mix(parts, residual_in, norm_gain.reshape(1, width), slots)
    outgoing = outgoing.reshape(experts, capacity, width)
    arrived = lax.all_to_all(outgoing, ("sp", "tp"), split_axis=0, concat_axis=0, tiled=True)
    result = expert(arrived.reshape(-1, width), expert_gate, expert_up, expert_down)
    result = result.reshape(experts, capacity, width)
    returned = lax.all_to_all(result, ("sp", "tp"), split_axis=0, concat_axis=0, tiled=True)
    return collect(returned.reshape(-1, width), weights, resid)


def solution(mesh):
    in_specs = (
        P(("grp", "sp", "tp"), None),
        P(("grp", "sp"), "tp"),
        P(("grp", "sp"), "tp"),
        P(None, ("grp", "sp")),
        P(None, ("grp", "sp")),
        P(None, ("grp", "sp")),
        P(None, ("grp", "sp")),
        P("tp", ("grp", "sp")),
        P("tp", ("grp", "sp")),
        P("tp", None),
        P("tp", None),
        P(),
        P(("sp", "tp"), None, None),
        P(("sp", "tp"), None, None),
        P(("sp", "tp"), None, None),
        P(("grp", "sp", "tp"), None),
        P(("grp", "sp", "tp"), None),
    )
    out_specs = P(("grp", "sp", "tp"), None)

    return jax.shard_map(shards, mesh=mesh, in_specs=in_specs, out_specs=out_specs, check_vma=False)
```

profile of v0, /device:TPU:33, one launch (start us, length us, event | category | flops | bytes accessed | tf_op | source)
XLA Modules:
  0.0 265.6 jit_solution(9355654364397392693)
XLA Ops:
  1.6 20.5 %collective-permute-start.9 = (bf16[416,256]{1,0:T(8,128)(2,1)S(1)}, bf16[416,256]{1,0:T(8,128)(2,1)S(1)}, u32[]{:S(2)}, u32[]{:S(2)}) collective-permute-start(bf16[416,256]{1,0:T(8,128)(2,1)S(1)} %packed.1.block), channel_id=1, source_target_pairs={{0,4},{4,0},{8,12},{12,8},{16,20},{20,16},{24,28},{28,24},{32,36},... | collective-permute-start | bytes 638984 | tf_op jit(solution)/shard_map/ppermute | solution.py:222
  22.2 3.1 %collective-permute-start.1 = (bf16[416,256]{1,0:T(8,128)(2,1)S(1)}, bf16[416,256]{1,0:T(8,128)(2,1)S(1)}, u32[]{:S(2)}, u32[]{:S(2)}) collective-permute-start(bf16[416,256]{1,0:T(8,128)(2,1)S(1)} %packed.1.block), channel_id=1, source_target_pairs={{0,8},{4,124},{8,16},{12,4},{16,24},{20,12},{24,32},{28,20},{32,40... | collective-permute-start | bytes 638984 | tf_op jit(solution)/shard_map/ppermute | solution.py:226
  28.1 3.1 %collective-permute-start.2 = (bf16[416,256]{1,0:T(8,128)(2,1)S(1)}, bf16[416,256]{1,0:T(8,128)(2,1)S(1)}, u32[]{:S(2)}, u32[]{:S(2)}) collective-permute-start(bf16[416,256]{1,0:T(8,128)(2,1)S(1)} %collective-permute-done.1.refs_0_), channel_id=1, source_target_pairs={{0,8},{4,124},{8,16},{12,4},{16,24},{20,12},{24,32},{28,20},{32,40... | collective-permute-start | bytes 638984 | tf_op jit(solution)/shard_map/ppermute | solution.py:226
  31.2 2.3 collective-permute-start.11
  34.0 3.1 %collective-permute-start.3 = (bf16[416,256]{1,0:T(8,128)(2,1)S(1)}, bf16[416,256]{1,0:T(8,128)(2,1)S(1)}, u32[]{:S(2)}, u32[]{:S(2)}) collective-permute-start(bf16[416,256]{1,0:T(8,128)(2,1)S(1)} %collective-permute-done.2.refs_0_), channel_id=1, source_target_pairs={{0,8},{4,124},{8,16},{12,4},{16,24},{20,12},{24,32},{28,20},{32,40... | collective-permute-start | bytes 638984 | tf_op jit(solution)/shard_map/ppermute | solution.py:226
  37.1 2.3 collective-permute-start.12
  39.9 3.1 %collective-permute-start.4 = (bf16[416,256]{1,0:T(8,128)(2,1)S(1)}, bf16[416,256]{1,0:T(8,128)(2,1)S(1)}, u32[]{:S(2)}, u32[]{:S(2)}) collective-permute-start(bf16[416,256]{1,0:T(8,128)(2,1)S(1)} %collective-permute-done.3.refs_0_), channel_id=1, source_target_pairs={{0,8},{4,124},{8,16},{12,4},{16,24},{20,12},{24,32},{28,20},{32,40... | collective-permute-start | bytes 638984 | tf_op jit(solution)/shard_map/ppermute | solution.py:226
  43.0 2.3 collective-permute-start.13
  45.8 3.1 %collective-permute-start.5 = (bf16[416,256]{1,0:T(8,128)(2,1)S(1)}, bf16[416,256]{1,0:T(8,128)(2,1)S(1)}, u32[]{:S(2)}, u32[]{:S(2)}) collective-permute-start(bf16[416,256]{1,0:T(8,128)(2,1)S(1)} %collective-permute-done.4.refs_0_), channel_id=1, source_target_pairs={{0,8},{4,124},{8,16},{12,4},{16,24},{20,12},{24,32},{28,20},{32,40... | collective-permute-start | bytes 638984 | tf_op jit(solution)/shard_map/ppermute | solution.py:226
  48.9 2.3 collective-permute-start.14
  51.7 3.1 %collective-permute-start.6 = (bf16[416,256]{1,0:T(8,128)(2,1)S(1)}, bf16[416,256]{1,0:T(8,128)(2,1)S(1)}, u32[]{:S(2)}, u32[]{:S(2)}) collective-permute-start(bf16[416,256]{1,0:T(8,128)(2,1)S(1)} %collective-permute-done.5.refs_0_), channel_id=1, source_target_pairs={{0,8},{4,124},{8,16},{12,4},{16,24},{20,12},{24,32},{28,20},{32,40... | collective-permute-start | bytes 638984 | tf_op jit(solution)/shard_map/ppermute | solution.py:226
  54.8 2.3 collective-permute-start.15
  57.6 3.1 %collective-permute-start.7 = (bf16[416,256]{1,0:T(8,128)(2,1)S(1)}, bf16[416,256]{1,0:T(8,128)(2,1)S(1)}, u32[]{:S(2)}, u32[]{:S(2)}) collective-permute-start(bf16[416,256]{1,0:T(8,128)(2,1)S(1)} %collective-permute-done.6.refs_0_), channel_id=1, source_target_pairs={{0,8},{4,124},{8,16},{12,4},{16,24},{20,12},{24,32},{28,20},{32,40... | collective-permute-start | bytes 638984 | tf_op jit(solution)/shard_map/ppermute | solution.py:226
  62.6 4.2 %collective-permute-start = (bf16[256,512]{1,0:T(8,128)(2,1)S(1)}, bf16[256,512]{1,0:T(8,128)(2,1)S(1)}, u32[]{:S(2)}, u32[]{:S(2)}) collective-permute-start(bf16[256,512]{1,0:T(8,128)(2,1)S(1)} %constant_dynamic-update-slice_fusion.own), channel_id=1, source_target_pairs={{0,4},{4,0},{8,12},{12,8},{16,20},{20,16},{24,28},{28,24},{32,36},... | collective-permute-start | bytes 786440 | tf_op jit(solution)/shard_map/ppermute | solution.py:221
  66.8 3.0 %collective-permute-start.16 = (bf16[416,256]{1,0:T(8,128)(2,1)S(1)}, bf16[416,256]{1,0:T(8,128)(2,1)S(1)}, u32[]{:S(2)}, u32[]{:S(2)}) collective-permute-start(bf16[416,256]{1,0:T(8,128)(2,1)S(1)} %collective-permute-done.15.refs_1_), channel_id=1, source_target_pairs={{0,8},{4,124},{8,16},{12,4},{16,24},{20,12},{24,32},{28,20},{32,40... | collective-permute-start | bytes 638984 | tf_op jit(solution)/shard_map/ppermute | solution.py:229
  70.0 2.8 %first.1 = (bf16[6,144,256]{2,1,0:T(8,128)(2,1)S(1)}, bf16[6,144,256]{2,1,0:T(8,128)(2,1)S(1)}, f32[2,6,152,256]{3,2,1,0:T(8,128)S(1)}) custom-call(s32[9]{0:T(128)S(1)} %pad_add_fusion.info.flags, bf16[256,512]{1,0:T(8,128)(2,1)S(1)} %constant_dynamic-update-slice_fusion.own, bf16[256,512]{1,0:T(8,128)(2,1)S(1)} %collective-permute-done.peer, ...), custom_call_target="tpu_custom_call" | custom-call | tf_op jit(solution)/shard_map/first/pallas_call | solution.py:141
  77.4 2.3 collective-permute-start.17
  79.7 2.1 collective-permute-done.17.got
  83.6 4.4 %all-to-all-start = ((bf16[4,64,2048]{2,1,0:T(8,128)(2,1)}), bf16[4,64,2048]{2,1,0:T(8,128)(2,1)S(1)}, u32[]{:S(2)}, u32[]{:S(2)}) async-start(bf16[4,64,2048]{2,1,0:T(8,128)(2,1)} %bitcast.2), calls=%async_computation | async-start | bytes 2097152 | tf_op jit(solution)/shard_map/all_to_all | solution.py:396
  89.0 13.6 %all-to-all-done.parts = bf16[4,64,2048]{2,1,0:T(8,128)(2,1)S(1)} async-done(((bf16[4,64,2048]{2,1,0:T(8,128)(2,1)}), bf16[4,64,2048]{2,1,0:T(8,128)(2,1)S(1)}, u32[]{:S(2)}, u32[]{:S(2)}) %all-to-all-start) | async-done | bytes 1048608 | tf_op jit(solution)/shard_map/all_to_all | solution.py:396
  104.0 89.0 %all_to_all.15 = bf16[128,2,2048]{2,1,0:T(2,128)(2,1)S(1)} all-to-all(bf16[128,2,2048]{2,1,0:T(2,128)(2,1)S(1)} %reshape.70), channel_id=1, replica_groups=mesh['grp'=2,'sp'=32,'tp'=4] {'sp','tp'}, dimensions={0} | all-to-all | bytes 2097152 | tf_op jit(solution)/shard_map/all_to_all | solution.py:399
  193.4 4.9 %expert.1 = bf16[256,2048]{1,0:T(8,128)(2,1)S(1)} custom-call(bf16[256,2048]{1,0:T(8,128)(2,1)S(1)} %reshape.71.rows, bf16[1,2048,512]{2,1,0:T(8,128)(2,1)} %gate.1, bf16[1,2048,512]{2,1,0:T(8,128)(2,1)} %up.1, bf16[1,512,2048]{2,1,0:T(8,128)(2,1)} %down.1), custom_call_target="tpu_custom_call" | custom-call | tf_op jit(solution)/shard_map/expert/pallas_call | solution.py:303
  199.9 8.5 %all-to-all-start.2 = ((bf16[128,2,2048]{2,1,0:T(2,128)(2,1)}), bf16[128,2,2048]{2,1,0:T(2,128)(2,1)}, u32[]{:S(2)}, u32[]{:S(2)}) async-start(bf16[128,2,2048]{2,1,0:T(2,128)(2,1)} %reshape.72), calls=%async_computation.2 | async-start | bytes 2097152 | tf_op jit(solution)/shard_map/all_to_all | solution.py:402
  208.5 54.2 %all-to-all-done.2 = bf16[128,2,2048]{2,1,0:T(2,128)(2,1)} async-done(((bf16[128,2,2048]{2,1,0:T(2,128)(2,1)}), bf16[128,2,2048]{2,1,0:T(2,128)(2,1)}, u32[]{:S(2)}, u32[]{:S(2)}) %all-to-all-start.2) | async-done | bytes 1048608 | tf_op jit(solution)/shard_map/all_to_all | solution.py:402
  (67 shorter events, 22.4 us)
Async XLA Ops:
  1.6 23.6 %collective-permute-start.9 = (bf16[416,256]{1,0:T(8,128)(2,1)S(1)}, bf16[416,256]{1,0:T(8,128)(2,1)S(1)}, u32[]{:S(2)}, u32[]{:S(2)}) collective-permute-start(bf16[416,256]{1,0:T(8,128)(2,1)S(1)} %packed.1.block), channel_id=1, source_target_pairs={{0,4},{4,0},{8,12},{12,8},{16,20},{20,16},{24,28},{28,24},{32,36},... | collective-permute-start | bytes 638984 | tf_op jit(solution)/shard_map/ppermute | solution.py:222
  22.2 5.9 %collective-permute-start.1 = (bf16[416,256]{1,0:T(8,128)(2,1)S(1)}, bf16[416,256]{1,0:T(8,128)(2,1)S(1)}, u32[]{:S(2)}, u32[]{:S(2)}) collective-permute-start(bf16[416,256]{1,0:T(8,128)(2,1)S(1)} %packed.1.block), channel_id=1, source_target_pairs={{0,8},{4,124},{8,16},{12,4},{16,24},{20,12},{24,32},{28,20},{32,40... | collective-permute-start | bytes 638984 | tf_op jit(solution)/shard_map/ppermute | solution.py:226
  25.3 5.9 %collective-permute-start.10 = (bf16[416,256]{1,0:T(8,128)(2,1)S(1)}, bf16[416,256]{1,0:T(8,128)(2,1)S(1)}, u32[]{:S(2)}, u32[]{:S(2)}) collective-permute-start(bf16[416,256]{1,0:T(8,128)(2,1)S(1)} %collective-permute-done.9), channel_id=1, source_target_pairs={{0,8},{4,124},{8,16},{12,4},{16,24},{20,12},{24,32},{28,20},{32,40... | collective-permute-start | bytes 638984 | tf_op jit(solution)/shard_map/ppermute | solution.py:229
  28.1 5.9 %collective-permute-start.2 = (bf16[416,256]{1,0:T(8,128)(2,1)S(1)}, bf16[416,256]{1,0:T(8,128)(2,1)S(1)}, u32[]{:S(2)}, u32[]{:S(2)}) collective-permute-start(bf16[416,256]{1,0:T(8,128)(2,1)S(1)} %collective-permute-done.1.refs_0_), channel_id=1, source_target_pairs={{0,8},{4,124},{8,16},{12,4},{16,24},{20,12},{24,32},{28,20},{32,40... | collective-permute-start | bytes 638984 | tf_op jit(solution)/shard_map/ppermute | solution.py:226
  31.2 5.9 %collective-permute-start.11 = (bf16[416,256]{1,0:T(8,128)(2,1)S(1)}, bf16[416,256]{1,0:T(8,128)(2,1)S(1)}, u32[]{:S(2)}, u32[]{:S(2)}) collective-permute-start(bf16[416,256]{1,0:T(8,128)(2,1)S(1)} %collective-permute-done.10.refs_1_), channel_id=1, source_target_pairs={{0,8},{4,124},{8,16},{12,4},{16,24},{20,12},{24,32},{28,20},{32,40... | collective-permute-start | bytes 638984 | tf_op jit(solution)/shard_map/ppermute | solution.py:229
  34.0 5.9 %collective-permute-start.3 = (bf16[416,256]{1,0:T(8,128)(2,1)S(1)}, bf16[416,256]{1,0:T(8,128)(2,1)S(1)}, u32[]{:S(2)}, u32[]{:S(2)}) collective-permute-start(bf16[416,256]{1,0:T(8,128)(2,1)S(1)} %collective-permute-done.2.refs_0_), channel_id=1, source_target_pairs={{0,8},{4,124},{8,16},{12,4},{16,24},{20,12},{24,32},{28,20},{32,40... | collective-permute-start | bytes 638984 | tf_op jit(solution)/shard_map/ppermute | solution.py:226
  37.1 5.9 %collective-permute-start.12 = (bf16[416,256]{1,0:T(8,128)(2,1)S(1)}, bf16[416,256]{1,0:T(8,128)(2,1)S(1)}, u32[]{:S(2)}, u32[]{:S(2)}) collective-permute-start(bf16[416,256]{1,0:T(8,128)(2,1)S(1)} %collective-permute-done.11.refs_1_), channel_id=1, source_target_pairs={{0,8},{4,124},{8,16},{12,4},{16,24},{20,12},{24,32},{28,20},{32,40... | collective-permute-start | bytes 638984 | tf_op jit(solution)/shard_map/ppermute | solution.py:229
  39.9 5.9 %collective-permute-start.4 = (bf16[416,256]{1,0:T(8,128)(2,1)S(1)}, bf16[416,256]{1,0:T(8,128)(2,1)S(1)}, u32[]{:S(2)}, u32[]{:S(2)}) collective-permute-start(bf16[416,256]{1,0:T(8,128)(2,1)S(1)} %collective-permute-done.3.refs_0_), channel_id=1, source_target_pairs={{0,8},{4,124},{8,16},{12,4},{16,24},{20,12},{24,32},{28,20},{32,40... | collective-permute-start | bytes 638984 | tf_op jit(solution)/shard_map/ppermute | solution.py:226
  43.0 5.9 %collective-permute-start.13 = (bf16[416,256]{1,0:T(8,128)(2,1)S(1)}, bf16[416,256]{1,0:T(8,128)(2,1)S(1)}, u32[]{:S(2)}, u32[]{:S(2)}) collective-permute-start(bf16[416,256]{1,0:T(8,128)(2,1)S(1)} %collective-permute-done.12.refs_1_), channel_id=1, source_target_pairs={{0,8},{4,124},{8,16},{12,4},{16,24},{20,12},{24,32},{28,20},{32,40... | collective-permute-start | bytes 638984 | tf_op jit(solution)/shard_map/ppermute | solution.py:229
  45.8 5.9 %collective-permute-start.5 = (bf16[416,256]{1,0:T(8,128)(2,1)S(1)}, bf16[416,256]{1,0:T(8,128)(2,1)S(1)}, u32[]{:S(2)}, u32[]{:S(2)}) collective-permute-start(bf16[416,256]{1,0:T(8,128)(2,1)S(1)} %collective-permute-done.4.refs_0_), channel_id=1, source_target_pairs={{0,8},{4,124},{8,16},{12,4},{16,24},{20,12},{24,32},{28,20},{32,40... | collective-permute-start | bytes 638984 | tf_op jit(solution)/shard_map/ppermute | solution.py:226
  48.9 5.9 %collective-permute-start.14 = (bf16[416,256]{1,0:T(8,128)(2,1)S(1)}, bf16[416,256]{1,0:T(8,128)(2,1)S(1)}, u32[]{:S(2)}, u32[]{:S(2)}) collective-permute-start(bf16[416,256]{1,0:T(8,128)(2,1)S(1)} %collective-permute-done.13.refs_1_), channel_id=1, source_target_pairs={{0,8},{4,124},{8,16},{12,4},{16,24},{20,12},{24,32},{28,20},{32,40... | collective-permute-start | bytes 638984 | tf_op jit(solution)/shard_map/ppermute | solution.py:229
  51.7 5.9 %collective-permute-start.6 = (bf16[416,256]{1,0:T(8,128)(2,1)S(1)}, bf16[416,256]{1,0:T(8,128)(2,1)S(1)}, u32[]{:S(2)}, u32[]{:S(2)}) collective-permute-start(bf16[416,256]{1,0:T(8,128)(2,1)S(1)} %collective-permute-done.5.refs_0_), channel_id=1, source_target_pairs={{0,8},{4,124},{8,16},{12,4},{16,24},{20,12},{24,32},{28,20},{32,40... | collective-permute-start | bytes 638984 | tf_op jit(solution)/shard_map/ppermute | solution.py:226
  54.8 12.0 %collective-permute-start.15 = (bf16[416,256]{1,0:T(8,128)(2,1)S(1)}, bf16[416,256]{1,0:T(8,128)(2,1)S(1)}, u32[]{:S(2)}, u32[]{:S(2)}) collective-permute-start(bf16[416,256]{1,0:T(8,128)(2,1)S(1)} %collective-permute-done.14.refs_1_), channel_id=1, source_target_pairs={{0,8},{4,124},{8,16},{12,4},{16,24},{20,12},{24,32},{28,20},{32,40... | collective-permute-start | bytes 638984 | tf_op jit(solution)/shard_map/ppermute | solution.py:229
  57.6 12.1 %collective-permute-start.7 = (bf16[416,256]{1,0:T(8,128)(2,1)S(1)}, bf16[416,256]{1,0:T(8,128)(2,1)S(1)}, u32[]{:S(2)}, u32[]{:S(2)}) collective-permute-start(bf16[416,256]{1,0:T(8,128)(2,1)S(1)} %collective-permute-done.6.refs_0_), channel_id=1, source_target_pairs={{0,8},{4,124},{8,16},{12,4},{16,24},{20,12},{24,32},{28,20},{32,40... | collective-permute-start | bytes 638984 | tf_op jit(solution)/shard_map/ppermute | solution.py:226
  62.6 7.4 %collective-permute-start = (bf16[256,512]{1,0:T(8,128)(2,1)S(1)}, bf16[256,512]{1,0:T(8,128)(2,1)S(1)}, u32[]{:S(2)}, u32[]{:S(2)}) collective-permute-start(bf16[256,512]{1,0:T(8,128)(2,1)S(1)} %constant_dynamic-update-slice_fusion.own), channel_id=1, source_target_pairs={{0,4},{4,0},{8,12},{12,8},{16,20},{20,16},{24,28},{28,24},{32,36},... | collective-permute-start | bytes 786440 | tf_op jit(solution)/shard_map/ppermute | solution.py:221
  66.8 9.3 %collective-permute-start.16 = (bf16[416,256]{1,0:T(8,128)(2,1)S(1)}, bf16[416,256]{1,0:T(8,128)(2,1)S(1)}, u32[]{:S(2)}, u32[]{:S(2)}) collective-permute-start(bf16[416,256]{1,0:T(8,128)(2,1)S(1)} %collective-permute-done.15.refs_1_), channel_id=1, source_target_pairs={{0,8},{4,124},{8,16},{12,4},{16,24},{20,12},{24,32},{28,20},{32,40... | collective-permute-start | bytes 638984 | tf_op jit(solution)/shard_map/ppermute | solution.py:229
  69.8 7.0 %collective-permute-start.8 = (bf16[416,256]{1,0:T(8,128)(2,1)S(1)}, bf16[416,256]{1,0:T(8,128)(2,1)S(1)}, u32[]{:S(2)}, u32[]{:S(2)}) collective-permute-start(bf16[416,256]{1,0:T(8,128)(2,1)S(1)} %collective-permute-done.7.refs_0_), channel_id=1, source_target_pairs={{0,8},{4,124},{8,16},{12,4},{16,24},{20,12},{24,32},{28,20},{32,40... | collective-permute-start | bytes 638984 | tf_op jit(solution)/shard_map/ppermute | solution.py:226
  76.7 5.1 %copy-start.1 = (bf16[256,2048]{1,0:T(8,128)(2,1)S(1)}, bf16[256,2048]{1,0:T(8,128)(2,1)}, u32[]{:S(2)}) copy-start(bf16[256,2048]{1,0:T(8,128)(2,1)} %project_l.1) | copy-start | bytes 3145732
  77.4 4.5 %collective-permute-start.17 = (f32[6,152,256]{2,1,0:T(8,128)S(1)}, f32[6,152,256]{2,1,0:T(8,128)S(1)}, u32[]{:S(2)}, u32[]{:S(2)}) collective-permute-start(f32[6,152,256]{2,1,0:T(8,128)S(1)} %slice_bitcast_fusion), channel_id=1, source_target_pairs={{0,4},{4,0},{8,12},{12,8},{16,20},{20,16},{24,28},{28,24},{32,36},... | collective-permute-start | bytes 2801672 | tf_op jit(solution)/shard_map/ppermute | solution.py:232
  83.6 5.3 %copy-start.3 = (bf16[2048]{0:T(1024)(128)(2,1)S(1)}, bf16[2048]{0:T(1024)(128)(2,1)}, u32[]{:S(2)}) copy-start(bf16[2048]{0:T(1024)(128)(2,1)} %param.28) | copy-start | bytes 12292
  83.6 19.0 %copy-start.2 = (bf16[64,2048]{1,0:T(8,128)(2,1)S(1)}, bf16[64,2048]{1,0:T(8,128)(2,1)}, u32[]{:S(2)}) copy-start(bf16[64,2048]{1,0:T(8,128)(2,1)} %residual_in.1) | copy-start | bytes 786436
  83.6 19.0 %all-to-all-start = ((bf16[4,64,2048]{2,1,0:T(8,128)(2,1)}), bf16[4,64,2048]{2,1,0:T(8,128)(2,1)S(1)}, u32[]{:S(2)}, u32[]{:S(2)}) async-start(bf16[4,64,2048]{2,1,0:T(8,128)(2,1)} %bitcast.2), calls=%async_computation | async-start | bytes 2097152 | tf_op jit(solution)/shard_map/all_to_all | solution.py:396
  198.3 10.0 %copy-start.5 = (f32[64,2]{0,1:T(2,128)S(1)}, f32[64,2]{0,1:T(2,128)}, u32[]{:S(2)}) copy-start(f32[64,2]{0,1:T(2,128)} %param.33) | copy-start | bytes 1540
  199.9 62.9 %all-to-all-start.2 = ((bf16[128,2,2048]{2,1,0:T(2,128)(2,1)}), bf16[128,2,2048]{2,1,0:T(2,128)(2,1)}, u32[]{:S(2)}, u32[]{:S(2)}) async-start(bf16[128,2,2048]{2,1,0:T(2,128)(2,1)} %reshape.72), calls=%async_computation.2 | async-start | bytes 2097152 | tf_op jit(solution)/shard_map/all_to_all | solution.py:402
  (2 other events, 9.0 us)
where the time goes:
time: 266 us
  blocking collectives  89 us (33%)
  starting transfers between devices  77.4 us (29%)
  waiting for transfers between devices  74.2 us (28%)
  Pallas kernels  16 us (6%)
  local copies, waits for them, and re-layouts  6.6 us (2%)
    all_to_all x1, blocking collectives, shards(): lax.all_to_all(outgoing, ('sp', 'tp'), split_axis=0, concat_axis=0, tiled...  89 us
    all_to_all x1, waiting for transfers between devices, shards(): lax.all_to_all(result, ('sp', 'tp'), split_axis=0, concat_axis=0, tiled=T...  54.2 us
    ppermute x8, starting transfers between devices, attend_and_project(): a = lax.ppermute(a, 'sp', ring)  21.9 us
    ppermute x1, starting transfers between devices, attend_and_project(): b = lax.ppermute(block, 'sp', swap)  20.5 us
    ppermute x7, starting transfers between devices, attend_and_project(): b = lax.ppermute(b, 'sp', ring)  15.4 us
    all_to_all x1, waiting for transfers between devices, shards(): parts = lax.all_to_all(parts, 'tp', split_axis=0, concat_axis=0, tiled=True)  13.6 us
    all_to_all x1, starting transfers between devices, shards(): lax.all_to_all(result, ('sp', 'tp'), split_axis=0, concat_axis=0, tiled=T...  8.49 us
  transfers between devices with their start and end apart: 20, of which 9 were waited for; matrix products, arithmetic and copies ran while one was open for 1% of the time, Pallas kernels for 3%

commit v1 on v0

--- a/solution.py
+++ b/solution.py
@@ -383,18 +383,20 @@
 
     capacity = max(2, 2 * own_rows * top_count // experts)
     pairs = own_rows * top_count
-    pair_expert = routing.reshape(-1)
+    gain = norm_gain.reshape(1, width)
+    pair_expert = (routing * capacity).reshape(-1)
     same = pair_expert[:, None] == pair_expert[None, :]
     before = jnp.arange(pairs)[:, None] > jnp.arange(pairs)[None, :]
     slot = jnp.sum((same & before).astype(jnp.int32), axis=1)
-    target = (pair_expert * capacity + slot).reshape(own_rows, top_count)
+    target = (pair_expert + slot).reshape(own_rows, top_count)
     hit = target[:, :, None] == jnp.arange(experts * capacity)[None, None, :]
     slots = jnp.any(hit, axis=1).T.astype(BF)
     weights = three_pieces(jnp.sum(jnp.where(hit, route_weight[:, :, None], 0.0), axis=1))
+    slots, weights = lax.optimization_barrier((slots, weights))
 
     parts = partial.reshape(head_devices, own_rows, width)
     parts = lax.all_to_all(parts, "tp", split_axis=0, concat_axis=0, tiled=True)
-    resid, outgoing = mix(parts, residual_in, norm_gain.reshape(1, width), slots)
+    resid, outgoing = mix(parts, residual_in, gain, slots)
     outgoing = outgoing.reshape(experts, capacity, width)
     arrived = lax.all_to_all(outgoing, ("sp", "tp"), split_axis=0, concat_axis=0, tiled=True)
     result = expert(arrived.reshape(-1, width), expert_gate, expert_up, expert_down)

time: 266 us -> 269 us (1.011)
  blocking collectives: 89 us -> 150 us
  waiting for transfers between devices: 74.2 us -> 19.2 us
  starting transfers between devices: 77.4 us -> 66.2 us
  local copies, waits for them, and re-layouts: 6.6 us -> 12.2 us
    all_to_all x0 -> x1, blocking collectives: none -> 62.6 us  [shards(): lax.all_to_all(result, ('sp', 'tp'), split_axis=0, concat_axis=0, tiled=T...]
    all_to_all x1 -> x0, waiting for transfers between devices: 54.2 us -> none  [shards(): lax.all_to_all(result, ('sp', 'tp'), split_axis=0, concat_axis=0, tiled=T...]
    all_to_all x1 -> x0, starting transfers between devices: 8.49 us -> none  [shards(): lax.all_to_all(result, ('sp', 'tp'), split_axis=0, concat_axis=0, tiled=T...]
    unnamed x14 -> x42, local copies, waits for them, and re-layouts: 1.04 us -> 7.51 us
  transfers between devices with their start and end apart: 20 -> 19, of which waited for: 9 -> 6; matrix products, arithmetic and copies ran while one was open for 1% -> 1% of each run, Pallas kernels for 3% -> 3%
where the time goes in v1:
time: 269 us; the launch traced here: 268 us
  blocking collectives  150 us (56%)
  starting transfers between devices  66.2 us (25%)
  waiting for transfers between devices  19.2 us (7%)
  Pallas kernels  17.9 us (7%)
  local copies, waits for them, and re-layouts  12.2 us (5%)
    all_to_all x1, blocking collectives, shards(): lax.all_to_all(outgoing, ('sp', 'tp'), split_axis=0, concat_axis=0, tiled...  87.6 us
    all_to_all x1, blocking collectives, shards(): lax.all_to_all(result, ('sp', 'tp'), split_axis=0, concat_axis=0, tiled=T...  62.6 us
    ppermute x8, starting transfers between devices, attend_and_project(): a = lax.ppermute(a, 'sp', ring)  21.5 us
    ppermute x1, starting transfers between devices, attend_and_project(): b = lax.ppermute(block, 'sp', swap)  20.5 us
    all_to_all x1, waiting for transfers between devices, shards(): parts = lax.all_to_all(parts, 'tp', split_axis=0, concat_axis=0, tiled=True)  14 us
    ppermute x7, starting transfers between devices, attend_and_project(): b = lax.ppermute(b, 'sp', ring)  13.3 us
    unnamed x42, local copies, waits for them, and re-layouts  7.51 us
  transfers between devices with their start and end apart: 19, of which 6 were waited for; matrix products, arithmetic and copies ran while one was open for 1% of the time, Pallas kernels for 3%

profile of v1, /device:TPU:33, one launch (start us, length us, event | category | flops | bytes accessed | tf_op | source)
XLA Modules:
  0.0 268.1 jit_solution(13933337452096714325)
XLA Ops:
  1.6 20.5 %collective-permute-start.9 = (bf16[416,256]{1,0:T(8,128)(2,1)S(1)}, bf16[416,256]{1,0:T(8,128)(2,1)S(1)}, u32[]{:S(2)}, u32[]{:S(2)}) collective-permute-start(bf16[416,256]{1,0:T(8,128)(2,1)S(1)} %packed.1.block), channel_id=1, source_target_pairs={{0,4},{4,0},{8,12},{12,8},{16,20},{20,16},{24,28},{28,24},{32,36},... | collective-permute-start | bytes 638984 | tf_op jit(solution)/shard_map/ppermute | solution.py:222
  22.2 3.1 %collective-permute-start.1 = (bf16[416,256]{1,0:T(8,128)(2,1)S(1)}, bf16[416,256]{1,0:T(8,128)(2,1)S(1)}, u32[]{:S(2)}, u32[]{:S(2)}) collective-permute-start(bf16[416,256]{1,0:T(8,128)(2,1)S(1)} %packed.1.block), channel_id=1, source_target_pairs={{0,8},{4,124},{8,16},{12,4},{16,24},{20,12},{24,32},{28,20},{32,40... | collective-permute-start | bytes 638984 | tf_op jit(solution)/shard_map/ppermute | solution.py:226
  26.4 1.7 collective-permute-done.1.refs_0_
  28.1 3.1 %collective-permute-start.2 = (bf16[416,256]{1,0:T(8,128)(2,1)S(1)}, bf16[416,256]{1,0:T(8,128)(2,1)S(1)}, u32[]{:S(2)}, u32[]{:S(2)}) collective-permute-start(bf16[416,256]{1,0:T(8,128)(2,1)S(1)} %collective-permute-done.1.refs_0_), channel_id=1, source_target_pairs={{0,8},{4,124},{8,16},{12,4},{16,24},{20,12},{24,32},{28,20},{32,40... | collective-permute-start | bytes 638984 | tf_op jit(solution)/shard_map/ppermute | solution.py:226
  31.2 2.3 collective-permute-start.11
  34.0 3.1 %collective-permute-start.3 = (bf16[416,256]{1,0:T(8,128)(2,1)S(1)}, bf16[416,256]{1,0:T(8,128)(2,1)S(1)}, u32[]{:S(2)}, u32[]{:S(2)}) collective-permute-start(bf16[416,256]{1,0:T(8,128)(2,1)S(1)} %collective-permute-done.2.refs_0_), channel_id=1, source_target_pairs={{0,8},{4,124},{8,16},{12,4},{16,24},{20,12},{24,32},{28,20},{32,40... | collective-permute-start | bytes 638984 | tf_op jit(solution)/shard_map/ppermute | solution.py:226
  37.1 2.3 collective-permute-start.12
  39.9 3.1 %collective-permute-start.4 = (bf16[416,256]{1,0:T(8,128)(2,1)S(1)}, bf16[416,256]{1,0:T(8,128)(2,1)S(1)}, u32[]{:S(2)}, u32[]{:S(2)}) collective-permute-start(bf16[416,256]{1,0:T(8,128)(2,1)S(1)} %collective-permute-done.3.refs_0_), channel_id=1, source_target_pairs={{0,8},{4,124},{8,16},{12,4},{16,24},{20,12},{24,32},{28,20},{32,40... | collective-permute-start | bytes 638984 | tf_op jit(solution)/shard_map/ppermute | solution.py:226
  43.7 1.6 collective-permute-start.13
  46.0 2.9 %collective-permute-start.5 = (bf16[416,256]{1,0:T(8,128)(2,1)S(1)}, bf16[416,256]{1,0:T(8,128)(2,1)S(1)}, u32[]{:S(2)}, u32[]{:S(2)}) collective-permute-start(bf16[416,256]{1,0:T(8,128)(2,1)S(1)} %collective-permute-done.4.refs_0_), channel_id=1, source_target_pairs={{0,8},{4,124},{8,16},{12,4},{16,24},{20,12},{24,32},{28,20},{32,40... | collective-permute-start | bytes 638984 | tf_op jit(solution)/shard_map/ppermute | solution.py:226
  51.9 2.9 %collective-permute-start.6 = (bf16[416,256]{1,0:T(8,128)(2,1)S(1)}, bf16[416,256]{1,0:T(8,128)(2,1)S(1)}, u32[]{:S(2)}, u32[]{:S(2)}) collective-permute-start(bf16[416,256]{1,0:T(8,128)(2,1)S(1)} %collective-permute-done.5.refs_0_), channel_id=1, source_target_pairs={{0,8},{4,124},{8,16},{12,4},{16,24},{20,12},{24,32},{28,20},{32,40... | collective-permute-start | bytes 638984 | tf_op jit(solution)/shard_map/ppermute | solution.py:226
  55.5 1.6 collective-permute-start.15
  57.6 3.1 %collective-permute-start.7 = (bf16[416,256]{1,0:T(8,128)(2,1)S(1)}, bf16[416,256]{1,0:T(8,128)(2,1)}, u32[]{:S(2)}, u32[]{:S(2)}) collective-permute-start(bf16[416,256]{1,0:T(8,128)(2,1)S(1)} %collective-permute-done.6.refs_0_), channel_id=1, source_target_pairs={{0,8},{4,124},{8,16},{12,4},{16,24},{20,12},{24,32},{28,20},{32,40... | collective-permute-start | bytes 638984 | tf_op jit(solution)/shard_map/ppermute | solution.py:226
  62.6 4.3 %collective-permute-start = (bf16[256,512]{1,0:T(8,128)(2,1)S(1)}, bf16[256,512]{1,0:T(8,128)(2,1)S(1)}, u32[]{:S(2)}, u32[]{:S(2)}) collective-permute-start(bf16[256,512]{1,0:T(8,128)(2,1)S(1)} %constant_dynamic-update-slice_fusion.own), channel_id=1, source_target_pairs={{0,4},{4,0},{8,12},{12,8},{16,20},{20,16},{24,28},{28,24},{32,36},... | collective-permute-start | bytes 786440 | tf_op jit(solution)/shard_map/ppermute | solution.py:221
  66.9 2.9 %collective-permute-start.16 = (bf16[416,256]{1,0:T(8,128)(2,1)}, bf16[416,256]{1,0:T(8,128)(2,1)S(1)}, u32[]{:S(2)}, u32[]{:S(2)}) collective-permute-start(bf16[416,256]{1,0:T(8,128)(2,1)} %collective-permute-done.15.refs_1_), channel_id=1, source_target_pairs={{0,8},{4,124},{8,16},{12,4},{16,24},{20,12},{24,32},{28,20},{32,40... | collective-permute-start | bytes 638984 | tf_op jit(solution)/shard_map/ppermute | solution.py:229
  70.0 2.8 %first.1 = (bf16[6,144,256]{2,1,0:T(8,128)(2,1)S(1)}, bf16[6,144,256]{2,1,0:T(8,128)(2,1)S(1)}, f32[2,6,152,256]{3,2,1,0:T(8,128)S(1)}) custom-call(s32[9]{0:T(128)S(1)} %pad_add_fusion.info.flags, bf16[256,512]{1,0:T(8,128)(2,1)S(1)} %constant_dynamic-update-slice_fusion.own, bf16[256,512]{1,0:T(8,128)(2,1)S(1)} %collective-permute-done.peer, ...), custom_call_target="tpu_custom_call" | custom-call | tf_op jit(solution)/shard_map/first/pallas_call | solution.py:141
  80.9 2.1 collective-permute-start.17
  83.6 1.9 collective-permute-done.17.got
  86.8 2.9 %finish.1 = bf16[256,2048]{1,0:T(8,128)(2,1)} custom-call(f32[2,6,152,256]{3,2,1,0:T(8,128)S(1)} %shard_map.170.state, f32[6,152,256]{2,1,0:T(8,128)} %collective-permute-done.17.got, bf16[256,2048]{1,0:T(8,128)(2,1)S(1)} %copy-done, bf16[256,2048]{1,0:T(8,128)(2,1)S(1)} %copy-done.1), custom_call_target="tpu_custom_call" | custom-call | tf_op jit(solution)/shard_map/finish/pallas_call | solution.py:195
  89.7 4.4 %all-to-all-start = ((bf16[4,64,2048]{2,1,0:T(8,128)(2,1)}), bf16[4,64,2048]{2,1,0:T(8,128)(2,1)S(1)}, u32[]{:S(2)}, u32[]{:S(2)}) async-start(bf16[4,64,2048]{2,1,0:T(8,128)(2,1)} %bitcast.2), calls=%async_computation | async-start | bytes 2097152 | tf_op jit(solution)/shard_map/all_to_all | solution.py:398
  94.6 14.0 %all-to-all-done.parts = bf16[4,64,2048]{2,1,0:T(8,128)(2,1)S(1)} async-done(((bf16[4,64,2048]{2,1,0:T(8,128)(2,1)}), bf16[4,64,2048]{2,1,0:T(8,128)(2,1)S(1)}, u32[]{:S(2)}, u32[]{:S(2)}) %all-to-all-start) | async-done | bytes 1048608 | tf_op jit(solution)/shard_map/all_to_all | solution.py:398
  110.1 87.6 %all_to_all.15 = bf16[128,2,2048]{2,1,0:T(2,128)(2,1)S(1)} all-to-all(bf16[128,2,2048]{2,1,0:T(2,128)(2,1)S(1)} %reshape.69), channel_id=1, replica_groups=mesh['grp'=2,'sp'=32,'tp'=4] {'sp','tp'}, dimensions={0} | all-to-all | bytes 2097152 | tf_op jit(solution)/shard_map/all_to_all | solution.py:401
  198.1 4.9 %expert.1 = bf16[256,2048]{1,0:T(8,128)(2,1)S(1)} custom-call(bf16[256,2048]{1,0:T(8,128)(2,1)S(1)} %reshape.70.rows, bf16[1,2048,512]{2,1,0:T(8,128)(2,1)} %gate.1, bf16[1,2048,512]{2,1,0:T(8,128)(2,1)} %up.1, bf16[1,512,2048]{2,1,0:T(8,128)(2,1)} %down.1), custom_call_target="tpu_custom_call" | custom-call | tf_op jit(solution)/shard_map/expert/pallas_call | solution.py:303
  203.7 62.6 %all_to_all.16 = bf16[128,2,2048]{2,1,0:T(2,128)(2,1)S(1)} all-to-all(bf16[128,2,2048]{2,1,0:T(2,128)(2,1)S(1)} %reshape.71), channel_id=1, replica_groups=mesh['grp'=2,'sp'=32,'tp'=4] {'sp','tp'}, dimensions={0} | all-to-all | bytes 2097152 | tf_op jit(solution)/shard_map/all_to_all | solution.py:404
  (95 shorter events, 25.9 us)
Async XLA Ops:
  1.6 23.6 %collective-permute-start.9 = (bf16[416,256]{1,0:T(8,128)(2,1)S(1)}, bf16[416,256]{1,0:T(8,128)(2,1)S(1)}, u32[]{:S(2)}, u32[]{:S(2)}) collective-permute-start(bf16[416,256]{1,0:T(8,128)(2,1)S(1)} %packed.1.block), channel_id=1, source_target_pairs={{0,4},{4,0},{8,12},{12,8},{16,20},{20,16},{24,28},{28,24},{32,36},... | collective-permute-start | bytes 638984 | tf_op jit(solution)/shard_map/ppermute | solution.py:222
  22.2 5.9 %collective-permute-start.1 = (bf16[416,256]{1,0:T(8,128)(2,1)S(1)}, bf16[416,256]{1,0:T(8,128)(2,1)S(1)}, u32[]{:S(2)}, u32[]{:S(2)}) collective-permute-start(bf16[416,256]{1,0:T(8,128)(2,1)S(1)} %packed.1.block), channel_id=1, source_target_pairs={{0,8},{4,124},{8,16},{12,4},{16,24},{20,12},{24,32},{28,20},{32,40... | collective-permute-start | bytes 638984 | tf_op jit(solution)/shard_map/ppermute | solution.py:226
  25.3 5.9 %collective-permute-start.10 = (bf16[416,256]{1,0:T(8,128)(2,1)S(1)}, bf16[416,256]{1,0:T(8,128)(2,1)S(1)}, u32[]{:S(2)}, u32[]{:S(2)}) collective-permute-start(bf16[416,256]{1,0:T(8,128)(2,1)S(1)} %collective-permute-done.9), channel_id=1, source_target_pairs={{0,8},{4,124},{8,16},{12,4},{16,24},{20,12},{24,32},{28,20},{32,40... | collective-permute-start | bytes 638984 | tf_op jit(solution)/shard_map/ppermute | solution.py:229
  28.1 5.9 %collective-permute-start.2 = (bf16[416,256]{1,0:T(8,128)(2,1)S(1)}, bf16[416,256]{1,0:T(8,128)(2,1)S(1)}, u32[]{:S(2)}, u32[]{:S(2)}) collective-permute-start(bf16[416,256]{1,0:T(8,128)(2,1)S(1)} %collective-permute-done.1.refs_0_), channel_id=1, source_target_pairs={{0,8},{4,124},{8,16},{12,4},{16,24},{20,12},{24,32},{28,20},{32,40... | collective-permute-start | bytes 638984 | tf_op jit(solution)/shard_map/ppermute | solution.py:226
  31.2 5.9 %collective-permute-start.11 = (bf16[416,256]{1,0:T(8,128)(2,1)S(1)}, bf16[416,256]{1,0:T(8,128)(2,1)S(1)}, u32[]{:S(2)}, u32[]{:S(2)}) collective-permute-start(bf16[416,256]{1,0:T(8,128)(2,1)S(1)} %collective-permute-done.10.refs_1_), channel_id=1, source_target_pairs={{0,8},{4,124},{8,16},{12,4},{16,24},{20,12},{24,32},{28,20},{32,40... | collective-permute-start | bytes 638984 | tf_op jit(solution)/shard_map/ppermute | solution.py:229
  34.0 5.9 %collective-permute-start.3 = (bf16[416,256]{1,0:T(8,128)(2,1)S(1)}, bf16[416,256]{1,0:T(8,128)(2,1)S(1)}, u32[]{:S(2)}, u32[]{:S(2)}) collective-permute-start(bf16[416,256]{1,0:T(8,128)(2,1)S(1)} %collective-permute-done.2.refs_0_), channel_id=1, source_target_pairs={{0,8},{4,124},{8,16},{12,4},{16,24},{20,12},{24,32},{28,20},{32,40... | collective-permute-start | bytes 638984 | tf_op jit(solution)/shard_map/ppermute | solution.py:226
  37.1 6.6 %collective-permute-start.12 = (bf16[416,256]{1,0:T(8,128)(2,1)S(1)}, bf16[416,256]{1,0:T(8,128)(2,1)S(1)}, u32[]{:S(2)}, u32[]{:S(2)}) collective-permute-start(bf16[416,256]{1,0:T(8,128)(2,1)S(1)} %collective-permute-done.11.refs_1_), channel_id=1, source_target_pairs={{0,8},{4,124},{8,16},{12,4},{16,24},{20,12},{24,32},{28,20},{32,40... | collective-permute-start | bytes 638984 | tf_op jit(solution)/shard_map/ppermute | solution.py:229
  39.9 6.1 %collective-permute-start.4 = (bf16[416,256]{1,0:T(8,128)(2,1)S(1)}, bf16[416,256]{1,0:T(8,128)(2,1)S(1)}, u32[]{:S(2)}, u32[]{:S(2)}) collective-permute-start(bf16[416,256]{1,0:T(8,128)(2,1)S(1)} %collective-permute-done.3.refs_0_), channel_id=1, source_target_pairs={{0,8},{4,124},{8,16},{12,4},{16,24},{20,12},{24,32},{28,20},{32,40... | collective-permute-start | bytes 638984 | tf_op jit(solution)/shard_map/ppermute | solution.py:226
  43.7 5.9 %collective-permute-start.13 = (bf16[416,256]{1,0:T(8,128)(2,1)S(1)}, bf16[416,256]{1,0:T(8,128)(2,1)S(1)}, u32[]{:S(2)}, u32[]{:S(2)}) collective-permute-start(bf16[416,256]{1,0:T(8,128)(2,1)S(1)} %collective-permute-done.12.refs_1_), channel_id=1, source_target_pairs={{0,8},{4,124},{8,16},{12,4},{16,24},{20,12},{24,32},{28,20},{32,40... | collective-permute-start | bytes 638984 | tf_op jit(solution)/shard_map/ppermute | solution.py:229
  46.0 5.9 %collective-permute-start.5 = (bf16[416,256]{1,0:T(8,128)(2,1)S(1)}, bf16[416,256]{1,0:T(8,128)(2,1)S(1)}, u32[]{:S(2)}, u32[]{:S(2)}) collective-permute-start(bf16[416,256]{1,0:T(8,128)(2,1)S(1)} %collective-permute-done.4.refs_0_), channel_id=1, source_target_pairs={{0,8},{4,124},{8,16},{12,4},{16,24},{20,12},{24,32},{28,20},{32,40... | collective-permute-start | bytes 638984 | tf_op jit(solution)/shard_map/ppermute | solution.py:226
  49.6 5.9 %collective-permute-start.14 = (bf16[416,256]{1,0:T(8,128)(2,1)S(1)}, bf16[416,256]{1,0:T(8,128)(2,1)S(1)}, u32[]{:S(2)}, u32[]{:S(2)}) collective-permute-start(bf16[416,256]{1,0:T(8,128)(2,1)S(1)} %collective-permute-done.13.refs_1_), channel_id=1, source_target_pairs={{0,8},{4,124},{8,16},{12,4},{16,24},{20,12},{24,32},{28,20},{32,40... | collective-permute-start | bytes 638984 | tf_op jit(solution)/shard_map/ppermute | solution.py:229
  51.9 5.7 %collective-permute-start.6 = (bf16[416,256]{1,0:T(8,128)(2,1)S(1)}, bf16[416,256]{1,0:T(8,128)(2,1)S(1)}, u32[]{:S(2)}, u32[]{:S(2)}) collective-permute-start(bf16[416,256]{1,0:T(8,128)(2,1)S(1)} %collective-permute-done.5.refs_0_), channel_id=1, source_target_pairs={{0,8},{4,124},{8,16},{12,4},{16,24},{20,12},{24,32},{28,20},{32,40... | collective-permute-start | bytes 638984 | tf_op jit(solution)/shard_map/ppermute | solution.py:226
  55.5 14.5 %copy-start.13 = (bf16[416,256]{1,0:T(8,128)(2,1)}, bf16[416,256]{1,0:T(8,128)(2,1)S(1)}, u32[]{:S(2)}) copy-start(bf16[416,256]{1,0:T(8,128)(2,1)S(1)} %collective-permute-done.14.refs_1_) | copy-start | bytes 638980
  55.5 11.4 %collective-permute-start.15 = (bf16[416,256]{1,0:T(8,128)(2,1)S(1)}, bf16[416,256]{1,0:T(8,128)(2,1)}, u32[]{:S(2)}, u32[]{:S(2)}) collective-permute-start(bf16[416,256]{1,0:T(8,128)(2,1)S(1)} %collective-permute-done.14.refs_1_), channel_id=1, source_target_pairs={{0,8},{4,124},{8,16},{12,4},{16,24},{20,12},{24,32},{28,20},{32,40... | collective-permute-start | bytes 638984 | tf_op jit(solution)/shard_map/ppermute | solution.py:229
  57.6 12.3 %copy-start.15 = (bf16[416,256]{1,0:T(8,128)(2,1)}, bf16[416,256]{1,0:T(8,128)(2,1)S(1)}, u32[]{:S(2)}) copy-start(bf16[416,256]{1,0:T(8,128)(2,1)S(1)} %collective-permute-done.6.refs_0_) | copy-start | bytes 638980
  57.6 12.1 %collective-permute-start.7 = (bf16[416,256]{1,0:T(8,128)(2,1)S(1)}, bf16[416,256]{1,0:T(8,128)(2,1)}, u32[]{:S(2)}, u32[]{:S(2)}) collective-permute-start(bf16[416,256]{1,0:T(8,128)(2,1)S(1)} %collective-permute-done.6.refs_0_), channel_id=1, source_target_pairs={{0,8},{4,124},{8,16},{12,4},{16,24},{20,12},{24,32},{28,20},{32,40... | collective-permute-start | bytes 638984 | tf_op jit(solution)/shard_map/ppermute | solution.py:226
  62.6 7.4 %collective-permute-start = (bf16[256,512]{1,0:T(8,128)(2,1)S(1)}, bf16[256,512]{1,0:T(8,128)(2,1)S(1)}, u32[]{:S(2)}, u32[]{:S(2)}) collective-permute-start(bf16[256,512]{1,0:T(8,128)(2,1)S(1)} %constant_dynamic-update-slice_fusion.own), channel_id=1, source_target_pairs={{0,4},{4,0},{8,12},{12,8},{16,20},{20,16},{24,28},{28,24},{32,36},... | collective-permute-start | bytes 786440 | tf_op jit(solution)/shard_map/ppermute | solution.py:221
  66.9 11.5 %collective-permute-start.16 = (bf16[416,256]{1,0:T(8,128)(2,1)}, bf16[416,256]{1,0:T(8,128)(2,1)S(1)}, u32[]{:S(2)}, u32[]{:S(2)}) collective-permute-start(bf16[416,256]{1,0:T(8,128)(2,1)} %collective-permute-done.15.refs_1_), channel_id=1, source_target_pairs={{0,8},{4,124},{8,16},{12,4},{16,24},{20,12},{24,32},{28,20},{32,40... | collective-permute-start | bytes 638984 | tf_op jit(solution)/shard_map/ppermute | solution.py:229
  69.8 9.6 %collective-permute-start.8 = (bf16[416,256]{1,0:T(8,128)(2,1)}, bf16[416,256]{1,0:T(8,128)(2,1)S(1)}, u32[]{:S(2)}, u32[]{:S(2)}) collective-permute-start(bf16[416,256]{1,0:T(8,128)(2,1)} %collective-permute-done.7.refs_0_), channel_id=1, source_target_pairs={{0,8},{4,124},{8,16},{12,4},{16,24},{20,12},{24,32},{28,20},{32,40... | collective-permute-start | bytes 638984 | tf_op jit(solution)/shard_map/ppermute | solution.py:226
  79.9 5.6 %copy-start = (bf16[256,2048]{1,0:T(8,128)(2,1)S(1)}, bf16[256,2048]{1,0:T(8,128)(2,1)}, u32[]{:S(2)}) copy-start(bf16[256,2048]{1,0:T(8,128)(2,1)} %project_s.1) | copy-start | bytes 3145732
  80.9 4.6 %collective-permute-start.17 = (f32[6,152,256]{2,1,0:T(8,128)}, f32[6,152,256]{2,1,0:T(8,128)}, u32[]{:S(2)}, u32[]{:S(2)}) collective-permute-start(f32[6,152,256]{2,1,0:T(8,128)} %slice_bitcast_fusion), channel_id=1, source_target_pairs={{0,4},{4,0},{8,12},{12,8},{16,20},{20,16},{24,28},{28,24},{32,36},... | collective-permute-start | bytes 2801672 | tf_op jit(solution)/shard_map/ppermute | solution.py:232
  89.7 4.9 %copy-start.17 = (bf16[2048]{0:T(1024)(128)(2,1)S(1)}, bf16[2048]{0:T(1024)(128)(2,1)}, u32[]{:S(2)}) copy-start(bf16[2048]{0:T(1024)(128)(2,1)} %param.28) | copy-start | bytes 12292
  89.7 19.0 %copy-start.2 = (bf16[64,2048]{1,0:T(8,128)(2,1)S(1)}, bf16[64,2048]{1,0:T(8,128)(2,1)}, u32[]{:S(2)}) copy-start(bf16[64,2048]{1,0:T(8,128)(2,1)} %residual_in.1) | copy-start | bytes 786436
  89.7 19.0 %all-to-all-start = ((bf16[4,64,2048]{2,1,0:T(8,128)(2,1)}), bf16[4,64,2048]{2,1,0:T(8,128)(2,1)S(1)}, u32[]{:S(2)}, u32[]{:S(2)}) async-start(bf16[4,64,2048]{2,1,0:T(8,128)(2,1)} %bitcast.2), calls=%async_computation | async-start | bytes 2097152 | tf_op jit(solution)/shard_map/all_to_all | solution.py:398
  (15 other events, 19.4 us)
